TPU v7x, 256 devices: a whole 4x4x8 slice. The times are simulated.
256 devices in a mesh: ep: 32 (over z, x), tp: 8 (over y, core).
Axes of the slice: x: 4, y: 4, z: 8, core: 2. Of those that a mesh axis runs over, the one named last changes fastest.
Arguments:
- stream: bfloat16 [8192, 3072], P('ep'), may hold values from -30 to 30
- ffn_gain: bfloat16 [3072], replicated, may hold values from 0.099609375 to 1.8984375
- chosen: int32 [32, 1024], replicated, may hold values from 0 to 8191, as said below
- affinity: float32 [32, 1024], P('ep'), may hold values from 0.5 to 2
- w_gate: bfloat16 [32, 3072, 3072], P('ep', None, 'tp'), may hold values from -0.109375 to 0.109375
- w_up: bfloat16 [32, 3072, 3072], P('ep', None, 'tp'), may hold values from -0.109375 to 0.109375
- w_down: bfloat16 [32, 3072, 3072], P('ep', 'tp'), may hold values from -0.109375 to 0.109375
- final_gain: bfloat16 [3072], P('tp'), may hold values from 0.099609375 to 1.8984375
Outputs:
- normed: bfloat16 [8192, 3072], P('ep', 'tp')
Inputs may be any that keep to these rules, and one draw needn't show every extreme that they name: `chosen`: row e holds 1024 distinct token numbers in ascending order. Of the 256 tokens of one index of ep, each expert reads at least one and at most 48; in every draw some expert reads exactly 48 from some index.
All inputs are finite; a program needn't handle non-finite values.
Results may differ from a plain program's by a relative error of at most 0.015.
Values may be sent and summed in bfloat16 or wider, within the bound.
A program may use at most 128 MiB of HBM per device.

v0:
```python
import jax
import jax.numpy as jnp
from jax import lax
from jax.sharding import PartitionSpec as P

EPSILON = 1e-06


def sent_to_all(array, axis):
    devices = lax.axis_size(axis)
    return lax.all_to_all(
        jnp.broadcast_to(array[None], (devices, *array.shape)), axis, 0, 0, tiled=True
    )


def over_copies(array, axis):
    return sent_to_all(array, axis).sum(axis=0)


def on_device(stream, ffn_gain, chosen, affinity, w_gate, w_up, w_down, final_gain):
    tok_rows = stream.shape[0]
    model_width = stream.shape[1]
    experts = chosen.shape[0]
    picks = chosen.shape[1]
    ep_count = lax.axis_size("ep")
    tp_count = lax.axis_size("tp")
    device = lax.axis_index("ep")
    column = lax.axis_index("tp")
    share_width = model_width // tp_count
    slots = 3 * tok_rows // 16
    widened = stream.astype(jnp.float32)
    scale_in = lax.rsqrt(jnp.mean(widened * widened, axis=-1, keepdims=True) + EPSILON)
    normed_in = (widened * scale_in * ffn_gain.astype(jnp.float32)).astype(jnp.bfloat16)
    source = chosen // tok_rows
    counts = jnp.sum(
        (source[:, :, None] == jnp.arange(ep_count)[None, None, :]).astype(jnp.int32), axis=1
    )
    starts = jnp.cumsum(counts, axis=1) - counts
    slot_range = jnp.arange(slots, dtype=jnp.int32)
    own_start = jnp.take(starts, device, axis=1)
    own_count = jnp.take(counts, device, axis=1)
    send_pos = jnp.clip(own_start[:, None] + slot_range[None, :], 0, picks - 1)
    send_valid = slot_range[None, :] < own_count[:, None]
    local_tok = jnp.where(
        send_valid, jnp.take_along_axis(chosen, send_pos, axis=1) - device * tok_rows, 0
    )
    local_flat = local_tok.reshape(-1)
    row_source = jnp.take(source, device, axis=0)
    row_starts = jnp.take(starts, device, axis=0)
    arrival = (
        row_source * slots + jnp.arange(picks, dtype=jnp.int32) - jnp.take(row_starts, row_source)
    )
    gate_rows = w_gate[0]
    up_rows = w_up[0]
    own_columns = lax.dynamic_slice_in_dim(normed_in, column * share_width, share_width, 1)
    outgoing = jnp.take(own_columns, local_flat, axis=0).reshape(experts, slots, share_width)
    arrived = lax.all_to_all(outgoing, "ep", split_axis=0, concat_axis=0, tiled=True)
    shared = jnp.take(arrived.reshape(-1, share_width), arrival, axis=0)
    piece = lax.all_gather(shared, "tp", axis=1, tiled=True)
    gate = jnp.dot(piece, gate_rows, preferred_element_type=jnp.float32)
    up = jnp.dot(piece, up_rows, preferred_element_type=jnp.float32)
    hidden = (jax.nn.silu(gate) * up).astype(jnp.bfloat16)
    down_rows = w_down[0]
    piece = down_rows
    expert_cols = lax.psum_scatter(
        lax.dot_general(
            piece, hidden, (((0,), (1,)), ((), ())), preferred_element_type=jnp.float32
        ).astype(jnp.bfloat16),
        "tp",
        scatter_dimension=0,
        tiled=True,
    ).astype(jnp.float32)
    weighted = (expert_cols * affinity[0][None, :]).astype(jnp.bfloat16)
    slot_pos = jnp.clip(row_starts[:, None] + slot_range[None, :], 0, picks - 1)
    leaving = jnp.take(weighted, slot_pos.reshape(-1), axis=1).reshape(share_width, ep_count, slots)
    returned = lax.all_to_all(leaving, "ep", split_axis=1, concat_axis=1, tiled=True)
    placing = (
        (local_flat[:, None] == jnp.arange(tok_rows, dtype=jnp.int32)[None, :])
        & send_valid.reshape(-1)[:, None]
    ).astype(jnp.bfloat16)
    update = lax.dot_general(
        placing,
        returned.reshape(share_width, -1),
        (((0,), (1,)), ((), ())),
        preferred_element_type=jnp.float32,
    )
    own_stream = lax.dynamic_slice_in_dim(widened, column * share_width, share_width, 1)
    merged = own_stream + update
    totals = over_copies(jnp.sum(merged * merged, axis=1), "tp")
    scale_out = lax.rsqrt(totals[:, None] / model_width + EPSILON)
    return (merged * scale_out * final_gain.astype(jnp.float32)[None, :]).astype(jnp.bfloat16)


def solution(mesh):
    return jax.shard_map(
        on_device,
        mesh=mesh,
        in_specs=(
            P("ep", None),
            P(),
            P(),
            P("ep", None),
            P("ep", None, "tp"),
            P("ep", None, "tp"),
            P("ep", "tp", None),
            P("tp"),
        ),
        out_specs=P("ep", "tp"),
        check_vma=False,
    )
```

profile of v0, /device:TPU:1, one launch (start us, length us, event | category | flops | bytes accessed | tf_op | source)
XLA Modules:
  0.0 273.2 jit_solution(4535225694800903247)
XLA Ops:
  6.5 2.0 multiply_reduce_fusion
  8.6 2.0 convert_element_type.34
  13.4 12.6 %gather_fusion.3 = s32[1536]{0:T(1024)S(1)} fusion(s32[32,1024]{1,0:T(8,128)S(1)} %copy-done.1, s32[1536]{0:T(1024)S(1)} %reshape.527), kind=kCustom, calls=%fused_computation.3 | custom fusion | bytes 24576 | tf_op jit(solution)/shard_map/jit(take_along_axis)/gather | solution.py:45
  28.3 5.3 %gather_fusion = bf16[1536,384]{1,0:T(8,128)(2,1)} fusion(bf16[256,384]{1,0:T(8,128)(2,1)S(1)} %multiply_convert_fusion.3, s32[2048]{0:T(1024)S(1)} %pad_clamp_fusion.1), kind=kCustom, calls=%fused_computation | custom fusion | bytes 2365440 | tf_op jit(solution)/shard_map/jit(_take)/gather | solution.py:56
  33.6 2.6 broadcast_select_fusion
  36.1 11.9 %all-to-all-start = ((bf16[32,48,384]{2,1,0:T(8,128)(2,1)}), bf16[32,48,384]{2,1,0:T(8,128)(2,1)S(1)}, u32[]{:S(2)}, u32[]{:S(2)}) async-start(bf16[32,48,384]{2,1,0:T(8,128)(2,1)} %broadcast_select_fusion), calls=%async_computation | async-start | bytes 2359296 | tf_op jit(solution)/shard_map/all_to_all | solution.py:57
  49.5 4.9 %compare_select_fusion.10 = (s32[1024,1]{0,1:T(1,128)S(1)}, s32[1024,1]{0,1:T(1,128)S(1)}, s32[1,1024]{1,0:T(1,128)S(1)}) fusion(s32[]{:T(128)} %bitcast.28, s32[]{:T(128)} %bitcast.29, s32[]{:T(128)} %bitcast.30, s32[]{:T(128)} %bitcast.31, s32[]{:T(128)} %bitcast.32, s32[]{:T(128)} %bitcast.34, s32[]{:T(128)} %bitcast.33, s32[32,1024]{1,0:T(8,128)} %copy-done.3, ...), kind=kLoop, calls=%fused_computation.80 | loop fusion | flops 16384 | bytes 16417 | tf_op jit(solution)/shard_map/jit(_take)/gather | solution.py:51
  55.3 16.2 %compare_and_fusion.2 = (pred[1024]{0:T(1024)(128)(4,1)}, s32[1024]{0:T(1024)S(1)}) fusion(s32[1024]{0:T(1024)S(1)} %bitcast.88, pred[1024]{0:T(1024)(128)(4,1)S(1)} %get-tuple-element.63, pred[1024]{0:T(1024)(128)(4,1)S(1)} %get-tuple-element.61, pred[1024]{0:T(1024)(128)(4,1)S(1)} %get-tuple-element.62, pred[1024]{0:T(1024)(128)(4,1)S(1)} %get-tuple-element.60, ...), kind=kLoop, calls=%fused_computation.101 | loop fusion | flops 41984 | bytes 39012 | tf_op jit(solution)/shard_map/jit(_take)/and | solution.py:58
  71.6 5.1 %all-to-all-done = bf16[32,48,384]{2,1,0:T(8,128)(2,1)S(1)} async-done(((bf16[32,48,384]{2,1,0:T(8,128)(2,1)}), bf16[32,48,384]{2,1,0:T(8,128)(2,1)S(1)}, u32[]{:S(2)}, u32[]{:S(2)}) %all-to-all-start) | async-done | bytes 1179680 | tf_op jit(solution)/shard_map/all_to_all | solution.py:57
  76.7 5.0 %gather_fusion.1 = bf16[1024,384]{1,0:T(8,128)(2,1)} fusion(bf16[1536,384]{1,0:T(8,128)(2,1)S(1)} %bitcast.84, s32[1024]{0:T(1024)S(1)} %broadcast_clamp_fusion), kind=kCustom, calls=%fused_computation.1 | custom fusion | bytes 1576960 | tf_op jit(solution)/shard_map/jit(_take)/gather | solution.py:58
  81.6 2.2 broadcast_select_fusion.2
  83.9 43.6 %all-gather.2.cloned.1.call-done = bf16[1024,3072]{1,0:T(8,128)(2,1)} async-done(((bf16[1024,384]{1,0:T(8,128)(2,1)}), bf16[1024,3072]{1,0:T(8,128)(2,1)}) %all-gather.2.cloned.1.call-update) | async-done | bytes 6291472 | tf_op jit(solution)/shard_map/all_gather | solution.py:59
  127.5 8.0 %fusion.3 = f32[1024,384]{1,0:T(8,128)} fusion(bf16[1024,3072]{1,0:T(8,128)(2,1)} %all-gather.2.cloned.1.call-done, bf16[1,3072,384]{2,1,0:T(8,128)(2,1)} %param.14), kind=kOutput, calls=%fused_computation.11 | convolution fusion | flops 2415919104 | bytes 10223616 | tf_op jit(solution)/shard_map/dot_general | solution.py:60
  135.5 11.4 %convert_bitcast_fusion = bf16[3072,1024]{0,1:T(8,128)(2,1)} fusion(bf16[1,384,3072]{2,1,0:T(8,128)(2,1)S(1)} %copy-done, f32[1024,384]{1,0:T(8,128)} %fusion.3, bf16[1024,3072]{1,0:T(8,128)(2,1)} %all-gather.2.cloned.1.call-done, bf16[1,3072,384]{2,1,0:T(8,128)(2,1)} %param.15), kind=kOutput, calls=%fused_computation.4 | convolution fusion | flops 4837343232 | bytes 18874368 | tf_op jit(solution)/shard_map/dot_general | solution.py:66
  146.9 8.7 %copy.10 = bf16[3072,1024]{1,0:T(8,128)(2,1)} copy(bf16[3072,1024]{0,1:T(8,128)(2,1)} %convert_bitcast_fusion) | data formatting | bytes 12582912
  156.6 43.4 %reduce-scatter.4.cloned.1.call-done = bf16[384,1024]{1,0:T(8,128)(2,1)} async-done(((bf16[3072,1024]{1,0:T(8,128)(2,1)}), bf16[384,1024]{1,0:T(8,128)(2,1)}) %reduce-scatter.4.cloned.1.call-update) | async-done | bytes 786448
  200.0 2.3 copy.11
  203.6 5.3 %gather_fusion.2 = bf16[1536,384]{1,0:T(8,128)(2,1)} fusion(bf16[384,1024]{0,1:T(8,128)(2,1)S(1)} %multiply_convert_fusion, s32[2048]{0:T(1024)S(1)} %pad_clamp_fusion), kind=kCustom, calls=%fused_computation.2 | custom fusion | bytes 2365440 | tf_op jit(solution)/shard_map/jit(_take)/gather | solution.py:75
  208.9 2.6 broadcast_select_fusion.1
  211.5 9.5 %all-to-all-start.1 = ((bf16[384,32,48]{0,2,1:T(8,128)(2,1)}), bf16[384,32,48]{0,2,1:T(8,128)(2,1)S(1)}, u32[]{:S(2)}, u32[]{:S(2)}) async-start(bf16[384,32,48]{0,2,1:T(8,128)(2,1)} %broadcast_select_fusion.1), calls=%async_computation.1 | async-start | bytes 2359296 | tf_op jit(solution)/shard_map/all_to_all | solution.py:76
  225.8 23.7 %all-to-all-done.1 = bf16[384,32,48]{0,2,1:T(8,128)(2,1)S(1)} async-done(((bf16[384,32,48]{0,2,1:T(8,128)(2,1)}), bf16[384,32,48]{0,2,1:T(8,128)(2,1)S(1)}, u32[]{:S(2)}, u32[]{:S(2)}) %all-to-all-start.1) | async-done | bytes 1179680 | tf_op jit(solution)/shard_map/all_to_all | solution.py:76
  249.5 2.9 %multiply_reduce_fusion.1 = (f32[256]{0:T(256)S(1)}, f32[256,384]{1,0:T(8,128)}) fusion(bf16[384,1536]{0,1:T(8,128)(2,1)S(1)} %bitcast.87, s32[1536]{0:T(1024)} %subtract_select_fusion, pred[1536]{0:T(1024)(128)(4,1)} %lt.182, f32[256,3072]{1,0:T(8,128)} %convert_element_type.34, s32[]{:T(128)S(6)} %select_n.231), kind=kOutput, calls=%fused_computation.25 | convolution fusion | flops 303070976 | bytes 1974788 | tf_op jit(solution)/shard_map/dot_general | solution.py:81
  253.0 7.0 %all-to-all-start.2 = ((f32[8,1,256]{2,1,0:T(1,128)}), f32[8,1,256]{2,1,0:T(1,128)S(1)}, u32[]{:S(2)}, u32[]{:S(2)}) async-start(f32[8,1,256]{2,1,0:T(1,128)} %broadcast_in_dim.111), calls=%async_computation.2 | async-start | bytes 16384 | tf_op jit(solution)/shard_map/all_to_all | solution.py:11
  260.0 4.6 %all-to-all-done.2 = f32[8,1,256]{2,1,0:T(1,128)S(1)} async-done(((f32[8,1,256]{2,1,0:T(1,128)}), f32[8,1,256]{2,1,0:T(1,128)S(1)}, u32[]{:S(2)}, u32[]{:S(2)}) %all-to-all-start.2) | async-done | bytes 8224 | tf_op jit(solution)/shard_map/all_to_all | solution.py:11
  (62 shorter events, 17.1 us)
Async XLA Ops:
  6.5 129.0 %copy-start = (bf16[1,384,3072]{2,1,0:T(8,128)(2,1)S(1)}, bf16[1,384,3072]{2,1,0:T(8,128)(2,1)}, u32[]{:S(2)}) copy-start(bf16[1,384,3072]{2,1,0:T(8,128)(2,1)} %param.16) | copy-start | bytes 7077892
  6.5 2.0 copy-start.2
  8.6 2.1 copy-start.1
  10.8 0.7 copy-start.3
  12.3 13.7 %copy-start.5 = (s32[32,32]{1,0:T(8,128)}, s32[32,32]{1,0:T(8,128)S(1)}, u32[]{:S(2)}) copy-start(s32[32,32]{1,0:T(8,128)S(1)} %sub.52) | copy-start | bytes 12292
  12.7 0.6 copy-start.4
  36.1 40.5 %all-to-all-start = ((bf16[32,48,384]{2,1,0:T(8,128)(2,1)}), bf16[32,48,384]{2,1,0:T(8,128)(2,1)S(1)}, u32[]{:S(2)}, u32[]{:S(2)}) async-start(bf16[32,48,384]{2,1,0:T(8,128)(2,1)} %broadcast_select_fusion), calls=%async_computation | async-start | bytes 2359296 | tf_op jit(solution)/shard_map/all_to_all | solution.py:57
  48.0 79.5 %all-gather.2.cloned.1.call-start = ((), (), s32[]{:S(2)}) async-start(), calls=%async_computation.4 | async-start | bytes 7077888 | tf_op jit(solution)/shard_map/all_gather | solution.py:59
  83.9 116.1 %reduce-scatter.4.cloned.1.call-start = ((), (), s32[]{:S(2)}) async-start(), calls=%async_computation.5 | async-start | bytes 7077888
  155.6 46.7 %copy-start.6 = (f32[1,1024]{1,0:T(1,128)S(1)}, f32[1,1024]{1,0:T(1,128)}, u32[]{:S(2)}) copy-start(f32[1,1024]{1,0:T(1,128)} %param.13) | copy-start | bytes 12292
  211.5 38.0 %all-to-all-start.1 = ((bf16[384,32,48]{0,2,1:T(8,128)(2,1)}), bf16[384,32,48]{0,2,1:T(8,128)(2,1)S(1)}, u32[]{:S(2)}, u32[]{:S(2)}) async-start(bf16[384,32,48]{0,2,1:T(8,128)(2,1)} %broadcast_select_fusion.1), calls=%async_computation.1 | async-start | bytes 2359296 | tf_op jit(solution)/shard_map/all_to_all | solution.py:76
  225.8 34.2 %copy-start.7 = (bf16[384]{0:T(512)(128)(2,1)S(1)}, bf16[384]{0:T(512)(128)(2,1)}, u32[]{:S(2)}) copy-start(bf16[384]{0:T(512)(128)(2,1)} %param.17) | copy-start | bytes 2308
  253.0 11.6 %all-to-all-start.2 = ((f32[8,1,256]{2,1,0:T(1,128)}), f32[8,1,256]{2,1,0:T(1,128)S(1)}, u32[]{:S(2)}, u32[]{:S(2)}) async-start(f32[8,1,256]{2,1,0:T(1,128)} %broadcast_in_dim.111), calls=%async_computation.2 | async-start | bytes 16384 | tf_op jit(solution)/shard_map/all_to_all | solution.py:11
Sparse Core Ops, SparseCore 0:
  84.0 43.4 all-gather.1
  155.7 44.2 reduce-scatter.3
where the time goes:
time: 275 us; the launch traced here: 273 us
  waiting for transfers between devices  120 us (44%)
  local copies, waits for them, and re-layouts  47.3 us (17%)
  other arithmetic  41.2 us (15%)
  starting transfers between devices  28.5 us (10%)
  matrix products  22.3 us (8%)
  between operations  13.6 us (5%)
    all_gather x1, waiting for transfers between devices, on_device(): piece = lax.all_gather(shared, 'tp', axis=1, tiled=True)  43.6 us
    unnamed x3, waiting for transfers between devices  43.4 us
    all_to_all x1, waiting for transfers between devices, on_device(): lax.all_to_all(leaving, 'ep', split_axis=1, concat_axis=1, tiled=True)  23.7 us
    and x1, other arithmetic, on_device(): shared = jnp.take(arrived.reshape(-1, share_width), arrival, axis=0)  16.2 us
    gather x3, local copies, waits for them, and re-layouts, on_device(): jnp.take_along_axis(chosen, send_pos, axis=1) - device * tok_rows  12.8 us
    unnamed x18, local copies, waits for them, and re-layouts  12.3 us
    all_to_all x1, starting transfers between devices, on_device(): lax.all_to_all(outgoing, 'ep', split_axis=0, concat_axis=0, tiled=True)  11.9 us
    dot_general x1, matrix products, on_device(): lax.dot_general(piece, hidden, (((0,), (1,)), ((), ())), preferred_elemen...  11.4 us
  transfers between devices with their start and end apart: 5, of which 5 were waited for; matrix products, arithmetic and copies ran while one was open for 11% of the time, Pallas kernels for 0%

commit v1 on v0

--- a/solution.py
+++ b/solution.py
@@ -1,9 +1,20 @@
+import functools
 import jax
 import jax.numpy as jnp
 from jax import lax
 from jax.sharding import PartitionSpec as P
 
 EPSILON = 1e-06
+
+
+def report_the_ranges(sheet, at_axis):
+    piece_out = jnp.concatenate(
+        lax.all_to_all(jnp.stack(lax.axis_size("tp") * [sheet], axis=0), "tp", 0, 0), at_axis
+    )
+    return piece_out
+
+
+create_rails_up = functools.partial(report_the_ranges, at_axis=1)
 
 
 def sent_to_all(array, axis):
@@ -56,7 +67,7 @@
     outgoing = jnp.take(own_columns, local_flat, axis=0).reshape(experts, slots, share_width)
     arrived = lax.all_to_all(outgoing, "ep", split_axis=0, concat_axis=0, tiled=True)
     shared = jnp.take(arrived.reshape(-1, share_width), arrival, axis=0)
-    piece = lax.all_gather(shared, "tp", axis=1, tiled=True)
+    piece = create_rails_up(shared)
     gate = jnp.dot(piece, gate_rows, preferred_element_type=jnp.float32)
     up = jnp.dot(piece, up_rows, preferred_element_type=jnp.float32)
     hidden = (jax.nn.silu(gate) * up).astype(jnp.bfloat16)

time: 275 us -> 307 us (1.12)
  blocking collectives: 0 us -> 78.6 us
  waiting for transfers between devices: 120 us -> 72.9 us
  local copies, waits for them, and re-layouts: 47.3 us -> 52.1 us
  matrix products: 22.3 us -> 19 us
    all_to_all x0 -> x1, blocking collectives: none -> 78.6 us  [report_the_ranges(): lax.all_to_all(jnp.stack(lax.axis_size('tp') * [sheet], axis=0), 'tp', 0, 0)]
    all_gather x1 -> x0, waiting for transfers between devices: 43.6 us -> none  [on_device(): piece = lax.all_gather(shared, 'tp', axis=1, tiled=True)]
    unnamed x3 -> x2, waiting for transfers between devices: 43.4 us -> 39.5 us
    dot_general x1, matrix products: 8.03 us -> 4.59 us  [on_device(): gate = jnp.dot(piece, gate_rows, preferred_element_type=jnp.float32)]
    unnamed x18 -> x22, local copies, waits for them, and re-layouts: 12.3 us -> 14.9 us
  transfers between devices with their start and end apart: 5 -> 4, of which waited for: 5 -> 4; matrix products, arithmetic and copies ran while one was open for 11% -> 10% of each run, Pallas kernels for 0% -> 0%
where the time goes in v1:
time: 307 us; the launch traced here: 306 us
  blocking collectives  78.6 us (26%)
  waiting for transfers between devices  72.9 us (24%)
  local copies, waits for them, and re-layouts  52.1 us (17%)
  other arithmetic  41.2 us (13%)
  starting transfers between devices  28.4 us (9%)
  matrix products  19 us (6%)
  between operations  13.6 us (4%)
    all_to_all x1, blocking collectives, report_the_ranges(): lax.all_to_all(jnp.stack(lax.axis_size('tp') * [sheet], axis=0), 'tp', 0, 0)  78.6 us
    unnamed x2, waiting for transfers between devices  39.5 us
    all_to_all x1, waiting for transfers between devices, on_device(): lax.all_to_all(leaving, 'ep', split_axis=1, concat_axis=1, tiled=True)  23.7 us
    and x1, other arithmetic, on_device(): shared = jnp.take(arrived.reshape(-1, share_width), arrival, axis=0)  16.2 us
    unnamed x22, local copies, waits for them, and re-layouts  14.9 us
    gather x3, local copies, waits for them, and re-layouts, on_device(): jnp.take_along_axis(chosen, send_pos, axis=1) - device * tok_rows  12.8 us
    all_to_all x1, starting transfers between devices, on_device(): lax.all_to_all(outgoing, 'ep', split_axis=0, concat_axis=0, tiled=True)  11.9 us
    dot_general x1, matrix products, on_device(): lax.dot_general(piece, hidden, (((0,), (1,)), ((), ())), preferred_elemen...  11.5 us
  transfers between devices with their start and end apart: 4, of which 4 were waited for; matrix products, arithmetic and copies ran while one was open for 10% of the time, Pallas kernels for 0%

profile of v1, /device:TPU:1, one launch (start us, length us, event | category | flops | bytes accessed | tf_op | source)
XLA Modules:
  0.0 305.9 jit_solution(17928445083725890768)
XLA Ops:
  8.6 2.0 convert_element_type.34
  13.4 12.6 %gather_fusion.3 = s32[1536]{0:T(1024)S(1)} fusion(s32[32,1024]{1,0:T(8,128)S(1)} %copy-done.1, s32[1536]{0:T(1024)S(1)} %reshape.542), kind=kCustom, calls=%fused_computation.3 | custom fusion | bytes 24576 | tf_op jit(solution)/shard_map/jit(take_along_axis)/gather | solution.py:56
  28.3 5.3 %gather_fusion = bf16[1536,384]{1,0:T(8,128)(2,1)} fusion(bf16[256,384]{1,0:T(8,128)(2,1)S(1)} %multiply_convert_fusion.3, s32[2048]{0:T(1024)S(1)} %pad_clamp_fusion.1), kind=kCustom, calls=%fused_computation | custom fusion | bytes 2365440 | tf_op jit(solution)/shard_map/jit(_take)/gather | solution.py:67
  33.6 2.6 broadcast_select_fusion
  36.1 11.9 %all-to-all-start = ((bf16[32,48,384]{2,1,0:T(8,128)(2,1)}), bf16[32,48,384]{2,1,0:T(8,128)(2,1)S(1)}, u32[]{:S(2)}, u32[]{:S(2)}) async-start(bf16[32,48,384]{2,1,0:T(8,128)(2,1)} %broadcast_select_fusion), calls=%async_computation | async-start | bytes 2359296 | tf_op jit(solution)/shard_map/all_to_all | solution.py:68
  49.5 4.9 %compare_select_fusion.10 = (s32[1024,1]{0,1:T(1,128)S(1)}, s32[1024,1]{0,1:T(1,128)S(1)}, s32[1,1024]{1,0:T(1,128)S(1)}) fusion(s32[]{:T(128)} %bitcast.28, s32[]{:T(128)} %bitcast.29, s32[]{:T(128)} %bitcast.30, s32[]{:T(128)} %bitcast.31, s32[]{:T(128)} %bitcast.32, s32[]{:T(128)} %bitcast.34, s32[]{:T(128)} %bitcast.33, s32[32,1024]{1,0:T(8,128)} %copy-done.5, ...), kind=kLoop, calls=%fused_computation.80 | loop fusion | flops 16384 | bytes 16417 | tf_op jit(solution)/shard_map/jit(_take)/gather | solution.py:62
  55.3 16.2 %compare_and_fusion.2 = (pred[1024]{0:T(1024)(128)(4,1)}, s32[1024]{0:T(1024)S(1)}) fusion(s32[1024]{0:T(1024)S(1)} %bitcast.93, pred[1024]{0:T(1024)(128)(4,1)S(1)} %get-tuple-element.63, pred[1024]{0:T(1024)(128)(4,1)S(1)} %get-tuple-element.61, pred[1024]{0:T(1024)(128)(4,1)S(1)} %get-tuple-element.62, pred[1024]{0:T(1024)(128)(4,1)S(1)} %get-tuple-element.60, ...), kind=kLoop, calls=%fused_computation.101 | loop fusion | flops 41984 | bytes 39012 | tf_op jit(solution)/shard_map/jit(_take)/and | solution.py:69
  71.6 5.1 %all-to-all-done = bf16[32,48,384]{2,1,0:T(8,128)(2,1)S(1)} async-done(((bf16[32,48,384]{2,1,0:T(8,128)(2,1)}), bf16[32,48,384]{2,1,0:T(8,128)(2,1)S(1)}, u32[]{:S(2)}, u32[]{:S(2)}) %all-to-all-start) | async-done | bytes 1179680 | tf_op jit(solution)/shard_map/all_to_all | solution.py:68
  76.7 5.0 %gather_fusion.1 = bf16[1024,384]{1,0:T(8,128)(2,1)} fusion(bf16[1536,384]{1,0:T(8,128)(2,1)S(1)} %bitcast.87, s32[1024]{0:T(1024)S(1)} %broadcast_clamp_fusion), kind=kCustom, calls=%fused_computation.1 | custom fusion | bytes 1576960 | tf_op jit(solution)/shard_map/jit(_take)/gather | solution.py:69
  81.6 2.2 broadcast_select_fusion.2
  86.1 78.6 %all_to_all.21 = bf16[8,1024,384]{1,2,0:T(8,128)(2,1)S(1)} all-to-all(bf16[8,1024,384]{1,2,0:T(8,128)(2,1)S(1)} %stack.2), channel_id=1, replica_groups=mesh['ep'=32,'tp'=8] {'tp'}, dimensions={0} | all-to-all | bytes 12582912 | tf_op jit(solution)/shard_map/all_to_all | solution.py:12
  164.7 2.7 copy-done.2
  167.3 4.6 %fusion.3 = f32[1024,384]{1,0:T(8,128)} fusion(bf16[1024,3072]{0,1:T(8,128)(2,1)S(1)} %bitcast.88, bf16[1,3072,384]{2,1,0:T(8,128)(2,1)S(1)} %copy-done.4), kind=kOutput, calls=%fused_computation.11 | convolution fusion | flops 2415919104 | bytes 10223616 | tf_op jit(solution)/shard_map/dot_general | solution.py:71
  171.9 11.5 %convert_bitcast_fusion = bf16[3072,1024]{0,1:T(8,128)(2,1)} fusion(bf16[1,384,3072]{2,1,0:T(8,128)(2,1)S(1)} %copy-done, f32[1024,384]{1,0:T(8,128)} %fusion.3, bf16[1024,3072]{0,1:T(8,128)(2,1)} %bitcast.89, bf16[1,3072,384]{2,1,0:T(8,128)(2,1)} %param.15), kind=kOutput, calls=%fused_computation.4 | convolution fusion | flops 4837343232 | bytes 18874368 | tf_op jit(solution)/shard_map/dot_general | solution.py:77
  183.5 8.6 %copy.14 = bf16[3072,1024]{1,0:T(8,128)(2,1)} copy(bf16[3072,1024]{0,1:T(8,128)(2,1)} %convert_bitcast_fusion) | data formatting | bytes 12582912
  193.1 39.5 %reduce-scatter.4.cloned.1.call-done = bf16[384,1024]{1,0:T(8,128)(2,1)} async-done(((bf16[3072,1024]{1,0:T(8,128)(2,1)}), bf16[384,1024]{1,0:T(8,128)(2,1)}) %reduce-scatter.4.cloned.1.call-update) | async-done | bytes 786448
  232.6 2.3 copy.15
  236.3 5.3 %gather_fusion.2 = bf16[1536,384]{1,0:T(8,128)(2,1)} fusion(bf16[384,1024]{0,1:T(8,128)(2,1)S(1)} %multiply_convert_fusion, s32[2048]{0:T(1024)S(1)} %pad_clamp_fusion), kind=kCustom, calls=%fused_computation.2 | custom fusion | bytes 2365440 | tf_op jit(solution)/shard_map/jit(_take)/gather | solution.py:86
  241.6 2.6 broadcast_select_fusion.1
  244.1 9.5 %all-to-all-start.2 = ((bf16[384,32,48]{0,2,1:T(8,128)(2,1)}), bf16[384,32,48]{0,2,1:T(8,128)(2,1)S(1)}, u32[]{:S(2)}, u32[]{:S(2)}) async-start(bf16[384,32,48]{0,2,1:T(8,128)(2,1)} %broadcast_select_fusion.1), calls=%async_computation.2 | async-start | bytes 2359296 | tf_op jit(solution)/shard_map/all_to_all | solution.py:87
  258.4 23.7 %all-to-all-done.2 = bf16[384,32,48]{0,2,1:T(8,128)(2,1)S(1)} async-done(((bf16[384,32,48]{0,2,1:T(8,128)(2,1)}), bf16[384,32,48]{0,2,1:T(8,128)(2,1)S(1)}, u32[]{:S(2)}, u32[]{:S(2)}) %all-to-all-start.2) | async-done | bytes 1179680 | tf_op jit(solution)/shard_map/all_to_all | solution.py:87
  282.1 2.9 multiply_reduce_fusion.1
  285.6 7.0 %all-to-all-start.3 = ((f32[8,1,256]{2,1,0:T(1,128)}), f32[8,1,256]{2,1,0:T(1,128)S(1)}, u32[]{:S(2)}, u32[]{:S(2)}) async-start(f32[8,1,256]{2,1,0:T(1,128)} %broadcast_in_dim.111), calls=%async_computation.3 | async-start | bytes 16384 | tf_op jit(solution)/shard_map/all_to_all | solution.py:22
  292.6 4.6 %all-to-all-done.3 = f32[8,1,256]{2,1,0:T(1,128)S(1)} async-done(((f32[8,1,256]{2,1,0:T(1,128)}), f32[8,1,256]{2,1,0:T(1,128)S(1)}, u32[]{:S(2)}, u32[]{:S(2)}) %all-to-all-start.3) | async-done | bytes 8224 | tf_op jit(solution)/shard_map/all_to_all | solution.py:22
  (66 shorter events, 21.2 us)
Async XLA Ops:
  6.5 165.4 %copy-start = (bf16[1,384,3072]{2,1,0:T(8,128)(2,1)S(1)}, bf16[1,384,3072]{2,1,0:T(8,128)(2,1)}, u32[]{:S(2)}) copy-start(bf16[1,384,3072]{2,1,0:T(8,128)(2,1)} %param.16) | copy-start | bytes 7077892
  6.5 2.0 copy-start.3
  8.6 2.1 copy-start.1
  10.8 0.7 copy-start.5
  12.3 13.7 %copy-start.7 = (s32[32,32]{1,0:T(8,128)}, s32[32,32]{1,0:T(8,128)S(1)}, u32[]{:S(2)}) copy-start(s32[32,32]{1,0:T(8,128)S(1)} %sub.52) | copy-start | bytes 12292
  12.7 0.6 copy-start.6
  36.1 40.5 %all-to-all-start = ((bf16[32,48,384]{2,1,0:T(8,128)(2,1)}), bf16[32,48,384]{2,1,0:T(8,128)(2,1)S(1)}, u32[]{:S(2)}, u32[]{:S(2)}) async-start(bf16[32,48,384]{2,1,0:T(8,128)(2,1)} %broadcast_select_fusion), calls=%async_computation | async-start | bytes 2359296 | tf_op jit(solution)/shard_map/all_to_all | solution.py:68
  48.0 184.6 %reduce-scatter.4.cloned.1.call-start = ((), (), s32[]{:S(2)}) async-start(), calls=%async_computation.5 | async-start | bytes 7077888
  86.1 81.3 %copy-start.4 = (bf16[1,3072,384]{2,1,0:T(8,128)(2,1)S(1)}, bf16[1,3072,384]{2,1,0:T(8,128)(2,1)}, u32[]{:S(2)}) copy-start(bf16[1,3072,384]{2,1,0:T(8,128)(2,1)} %param.14) | copy-start | bytes 7077892
  164.7 2.7 copy-start.2
  192.1 42.8 %copy-start.8 = (f32[1,1024]{1,0:T(1,128)S(1)}, f32[1,1024]{1,0:T(1,128)}, u32[]{:S(2)}) copy-start(f32[1,1024]{1,0:T(1,128)} %param.13) | copy-start | bytes 12292
  244.1 38.0 %all-to-all-start.2 = ((bf16[384,32,48]{0,2,1:T(8,128)(2,1)}), bf16[384,32,48]{0,2,1:T(8,128)(2,1)S(1)}, u32[]{:S(2)}, u32[]{:S(2)}) async-start(bf16[384,32,48]{0,2,1:T(8,128)(2,1)} %broadcast_select_fusion.1), calls=%async_computation.2 | async-start | bytes 2359296 | tf_op jit(solution)/shard_map/all_to_all | solution.py:87
  258.4 34.2 %copy-start.9 = (bf16[384]{0:T(512)(128)(2,1)S(1)}, bf16[384]{0:T(512)(128)(2,1)}, u32[]{:S(2)}) copy-start(bf16[384]{0:T(512)(128)(2,1)} %param.17) | copy-start | bytes 2308
  285.6 11.6 %all-to-all-start.3 = ((f32[8,1,256]{2,1,0:T(1,128)}), f32[8,1,256]{2,1,0:T(1,128)S(1)}, u32[]{:S(2)}, u32[]{:S(2)}) async-start(f32[8,1,256]{2,1,0:T(1,128)} %broadcast_in_dim.111), calls=%async_computation.3 | async-start | bytes 16384 | tf_op jit(solution)/shard_map/all_to_all | solution.py:22
Sparse Core Ops, SparseCore 0:
  192.2 40.3 reduce-scatter.3
